TPU v7x, 32 devices: a whole 2x2x4 slice. The times are simulated.
32 devices in a mesh: kv: 8 (over z, y), tp: 4 (over x, core).
Axes of the slice: x: 2, y: 2, z: 4, core: 2. Of those that a mesh axis runs over, the one named last changes fastest.
Arguments:
- tokens: bfloat16 [4, 4096], P(None, 'kv'), may hold values from -70 to 70
- norm_gain: float32 [4096], P('kv'), may hold values from 0.1 to 1.9
- query_weight: bfloat16 [4096, 2048], P('kv', 'tp'), may hold values from -0.09375 to 0.09375
- key_weight: bfloat16 [4096, 256], P('kv', 'tp'), may hold values from -0.09375 to 0.09375
- value_weight: bfloat16 [4096, 256], P('kv', 'tp'), may hold values from -0.09375 to 0.09375
- cache_keys: bfloat16 [4, 2, 6144, 128], P(None, None, ('kv', 'tp')), may hold values from -480 to 480, as said below
- cache_values: bfloat16 [4, 2, 6144, 128], P(None, None, ('kv', 'tp')), may hold values from -6 to 6
- lengths: int32 [4], replicated, may hold values from 1536 to 6143
- lambdas: float32 [16], P('tp'), may hold values from 0.3 to 0.8
- head_gain: float32 [128], replicated, may hold values from 0.1 to 1.9
- output_weight: bfloat16 [2048, 4096], P('tp', 'kv'), may hold values from -0.125 to 0.125
Outputs:
- attended: bfloat16 [4, 4096], P(None, 'kv')
- new_keys: bfloat16 [4, 256], P(None, 'tp')
- new_values: bfloat16 [4, 256], P(None, 'tp')
Inputs may be any that keep to these rules, and one draw needn't show every extreme that they name: `cache_keys`: of order 1.75 in most entries; some rows may be far larger.
All inputs are finite; a program needn't handle non-finite values.
Results may differ from a plain program's by a relative error of at most 0.038.
Values may be sent and summed in bfloat16 or wider, within the bound.
No kernel may reach another device: no remote copies, remote signals or barrier semaphores. Data moves between devices by JAX's collectives and lax.ppermute only.
A program may use at most 64 MiB of HBM per device.

v0:
```python
import jax
import jax.numpy as jnp
from jax import lax
from jax.sharding import PartitionSpec as P

D = 4096
HEADS = 16
KV_HEADS = 2
QK = 64
VD = 128
NEG_FILL = -1e30


def body(
    tokens,
    norm_gain,
    query_weight,
    key_weight,
    value_weight,
    cache_keys,
    cache_values,
    lengths,
    lambdas,
    head_gain,
    output_weight,
):
    floats = tokens.astype(jnp.float32)
    scaled = (floats * norm_gain).astype(jnp.bfloat16)
    query_part = jnp.dot(scaled, query_weight, preferred_element_type=jnp.float32)
    key_part = jnp.dot(scaled, key_weight, preferred_element_type=jnp.float32)
    value_part = jnp.dot(scaled, value_weight, preferred_element_type=jnp.float32)
    squares, query_sum, key_sum, value_sum = lax.psum(
        (jnp.sum(floats * floats, axis=1), query_part, key_part, value_part), "kv"
    )
    inverse = lax.rsqrt(squares / D + 1e-06)[:, None]
    queries = (query_sum * inverse).astype(jnp.bfloat16)
    new_keys = (key_sum * inverse).astype(jnp.bfloat16)
    new_values = (value_sum * inverse).astype(jnp.bfloat16)
    every_query = lax.all_gather(queries, "tp", axis=1, tiled=True)
    seq_count = tokens.shape[0]
    pos_count = cache_keys.shape[2]
    group_size = HEADS // KV_HEADS
    own_heads = lambdas.shape[0]
    first_position = (lax.axis_index("kv") * lax.axis_size("tp") + lax.axis_index("tp")) * pos_count
    positions = first_position + jnp.arange(pos_count, dtype=jnp.int32)
    live_mask = (positions[None, :] < lengths[:, None])[:, None, None, None, :]
    query_rows = every_query.reshape(seq_count, KV_HEADS, group_size, 2, QK)
    key_rows = cache_keys.reshape(seq_count, KV_HEADS, pos_count, 2, QK)
    scores = jnp.einsum(
        "bhgcd,bhpcd->bhgcp", query_rows, key_rows, preferred_element_type=jnp.float32
    ) * QK ** (-0.5)
    scores = jnp.where(live_mask, scores, NEG_FILL)
    local_peak = jnp.max(scores, axis=-1)
    peak_used = lax.pmax(local_peak, ("kv", "tp"))
    weights = jnp.where(live_mask, jnp.exp(scores - peak_used[..., None]), 0.0)
    totals = jnp.sum(weights, axis=-1).reshape(seq_count, HEADS, 2)
    summed = jnp.einsum(
        "bhgcp,bhpv->bhgcv",
        weights.astype(jnp.bfloat16),
        cache_values,
        preferred_element_type=jnp.float32,
    ).reshape(seq_count, HEADS, 2, VD)
    totals, summed = (
        lax.psum_scatter(totals.astype(jnp.bfloat16), "tp", scatter_dimension=1, tiled=True).astype(
            jnp.float32
        ),
        lax.psum_scatter(summed.astype(jnp.bfloat16), "tp", scatter_dimension=1, tiled=True).astype(
            jnp.float32
        ),
    )
    totals, summed = lax.psum((totals, summed), "kv")
    ratios = summed / totals[..., None]
    mixed = ratios[:, :, 0] - lambdas[None, :, None] * ratios[:, :, 1]
    normed = mixed * lax.rsqrt(jnp.mean(mixed * mixed, axis=-1, keepdims=True) + 1e-06) * head_gain
    flattened = normed.astype(jnp.bfloat16).reshape(seq_count, own_heads * VD)
    partial_out = jnp.dot(flattened, output_weight, preferred_element_type=jnp.float32)
    attended = lax.psum(partial_out.astype(jnp.bfloat16), "tp")
    return (attended, new_keys, new_values)


def solution(mesh):
    return jax.shard_map(
        body,
        mesh=mesh,
        in_specs=(
            P(None, "kv"),
            P("kv"),
            P("kv", "tp"),
            P("kv", "tp"),
            P("kv", "tp"),
            P(None, None, ("kv", "tp"), None),
            P(None, None, ("kv", "tp"), None),
            P(),
            P("tp"),
            P(),
            P("tp", "kv"),
        ),
        out_specs=(P(None, "kv"), P(None, "tp"), P(None, "tp")),
        check_vma=False,
    )
```

profile of v0, /device:TPU:0, one launch (start us, length us, event | category | flops | bytes accessed | tf_op | source)
XLA Modules:
  0.0 127.6 jit_solution(1251713564693285807)
XLA Ops:
  0.7 0.8 broadcast_compare_fusion
  1.5 0.2 copy-done
  1.7 0.9 fusion.24
  2.6 0.1 fusion.11
  2.8 23.6 %all-reduce.3 = (f32[4,512]{1,0:T(4,128)S(1)}, f32[4]{0:T(128)S(1)}) all-reduce(f32[4,512]{1,0:T(4,128)S(1)} %fusion.24, f32[4]{0:T(128)S(1)} %fusion.11), channel_id=1, replica_groups=mesh['kv'=8,'tp'=4] {'kv'}, use_global_device_ids=true, to_apply=%region_0.0 | all-reduce | flops 2052 | bytes 16416 | tf_op jit(solution)/shard_map/psum | solution.py:32
  26.5 5.2 %all_gather.3 = bf16[4,2048]{1,0:T(4,128)(2,1)S(1)} all-gather(bf16[4,512]{1,0:T(4,128)(2,1)S(1)} %multiply_convert_fusion), channel_id=1, replica_groups=mesh['kv'=8,'tp'=4] {'tp'}, dimensions={1}, use_global_device_ids=true | all-gather | bytes 20480 | tf_op jit(solution)/shard_map/all_gather | solution.py:39
  31.7 0.1 reshape.63
  31.8 0.2 copy.22
  32.0 0.3 fusion.27
  32.3 36.9 %pmax.7 = f32[4,2,8,2]{2,3,1,0:T(2,128)S(1)} all-reduce(f32[4,2,8,2]{2,3,1,0:T(2,128)S(1)} %get-tuple-element.15), channel_id=1, replica_groups=mesh['kv'=8,'tp'=4] {'kv','tp'}, use_global_device_ids=true, to_apply=%region_4.0 | all-reduce | flops 128 | bytes 1024 | tf_op jit(solution)/shard_map/pmax | solution.py:54
  69.2 0.2 fusion.3
  69.4 0.1 convert_element_type.51
  69.5 0.3 convolution_convert_fusion
  69.8 11.5 %all-reduce.4 = (bf16[4,16,2,128]{3,1,2,0:T(8,128)(2,1)S(1)}, bf16[4,16,2]{1,2,0:T(2,128)(2,1)S(1)}) all-reduce(bf16[4,16,2,128]{3,1,2,0:T(8,128)(2,1)S(1)} %bitcast.69, bf16[4,16,2]{1,2,0:T(2,128)(2,1)S(1)} %convert_element_type.51), channel_id=2, replica_groups=mesh['kv'=8,'tp'=4] {'tp'}, use_global_device_ids=true, to_apply=%region_5.6.clone | all-reduce | flops 16512 | bytes 66048
  81.4 0.6 dynamic-slice
  82.7 0.1 fusion.20
  82.8 0.1 fusion.22
  83.0 35.9 %all-reduce.2 = (f32[4,4,2,128]{3,1,2,0:T(4,128)S(1)}, f32[4,4,2]{1,2,0:T(2,128)S(1)}, f32[4,64]{1,0:T(4,128)S(1)}, f32[4,64]{1,0:T(4,128)S(1)}) all-reduce(f32[4,4,2,128]{3,1,2,0:T(4,128)S(1)} %dynamic-slice_convert_fusion, f32[4,4,2]{1,2,0:T(2,128)S(1)} %dynamic-slice_convert_fusion.1, ...), channel_id=1, replica_groups=mesh['kv'=8,'tp'=4] {'kv'}, use_global_device_ids=true, to_apply=%region_6.7 | all-reduce | flops 4640 | bytes 37120 | tf_op jit(solution)/shard_map/psum | solution.py:71
  118.9 0.6 multiply_convert_fusion.1
  119.7 0.6 copy-done.7
  120.3 0.2 fusion.16
  120.5 0.6 copy-done.8
  121.2 0.2 convolution_convert_fusion.1
  121.4 6.2 %psum.53 = bf16[4,512]{1,0:T(4,128)(2,1)} all-reduce(bf16[4,512]{1,0:T(4,128)(2,1)S(1)} %convolution_convert_fusion.1), channel_id=1, replica_groups=mesh['kv'=8,'tp'=4] {'tp'}, use_global_device_ids=true, to_apply=%region_11.12 | all-reduce | flops 2048 | bytes 8192 | tf_op jit(solution)/shard_map/psum | solution.py:77
  (31 shorter events, 0.5 us)
Async XLA Ops:
  0.6 1.1 copy-start
  0.6 31.1 %copy-start.2 = (bf16[4,2,192,128]{3,2,1,0:T(8,128)(2,1)S(1)}, bf16[4,2,192,128]{3,2,1,0:T(8,128)(2,1)}, u32[]{:S(2)}) copy-start(bf16[4,2,192,128]{3,2,1,0:T(8,128)(2,1)} %param.16) | copy-start | bytes 1179652
  1.7 0.9 copy-start.3
  32.0 37.5 %copy-start.9 = (bf16[4,2,192,128]{3,2,1,0:T(8,128)(2,1)S(1)}, bf16[4,2,192,128]{3,2,1,0:T(8,128)(2,1)}, u32[]{:S(2)}) copy-start(bf16[4,2,192,128]{3,2,1,0:T(8,128)(2,1)} %param.17) | copy-start | bytes 1179652
  69.5 51.7 %copy-start.1 = (bf16[512,512]{1,0:T(8,128)(2,1)S(1)}, bf16[512,512]{1,0:T(8,128)(2,1)}, u32[]{:S(2)}) copy-start(bf16[512,512]{1,0:T(8,128)(2,1)} %param.21) | copy-start | bytes 1572868
  69.7 11.6 %copy-start.10 = (u32[32]{0:T(128)S(1)}, u32[32]{0:T(128)}, u32[]{:S(2)}) copy-start(u32[32]{0:T(128)} %constant.32) | copy-start | bytes 388
  69.8 12.9 %copy-start.4 = (bf16[512,64]{0,1:T(8,128)(2,1)S(1)}, bf16[512,64]{0,1:T(8,128)(2,1)}, u32[]{:S(2)}) copy-start(bf16[512,64]{0,1:T(8,128)(2,1)} %param.15) | copy-start | bytes 196612
  69.8 12.9 %copy-start.6 = (f32[512]{0:T(512)S(1)}, f32[512]{0:T(512)}, u32[]{:S(2)}) copy-start(f32[512]{0:T(512)} %param.12) | copy-start | bytes 6148
  81.3 1.5 %copy-start.5 = (bf16[512,64]{0,1:T(8,128)(2,1)S(1)}, bf16[512,64]{0,1:T(8,128)(2,1)}, u32[]{:S(2)}) copy-start(bf16[512,64]{0,1:T(8,128)(2,1)} %param.14) | copy-start | bytes 196612
  119.6 0.7 copy-start.7
  120.5 0.7 copy-start.8
where the time goes:
time: 128 us
  blocking collectives  119 us (93%)
  local copies, waits for them, and re-layouts  2.65 us (2%)
  other arithmetic  2.17 us (2%)
  matrix products  1.87 us (1%)
  between operations  1.46 us (1%)
    pmax x1, blocking collectives, body(): peak_used = lax.pmax(local_peak, ('kv', 'tp'))  36.9 us
    psum x1, blocking collectives, body(): totals, summed = lax.psum((totals, summed), 'kv')  35.9 us
    psum x1, blocking collectives, body(): lax.psum((jnp.sum(floats * floats, axis=1), query_part, key_part, value_p...  23.6 us
    unnamed x1, blocking collectives  11.5 us
    psum x1, blocking collectives, body(): attended = lax.psum(partial_out.astype(jnp.bfloat16), 'tp')  6.24 us
    all_gather x1, blocking collectives, body(): every_query = lax.all_gather(queries, 'tp', axis=1, tiled=True)  5.19 us

commit v1 on v0

--- a/solution.py
+++ b/solution.py
@@ -36,7 +36,9 @@
     queries = (query_sum * inverse).astype(jnp.bfloat16)
     new_keys = (key_sum * inverse).astype(jnp.bfloat16)
     new_values = (value_sum * inverse).astype(jnp.bfloat16)
-    every_query = lax.all_gather(queries, "tp", axis=1, tiled=True)
+    tile_out = jnp.stack([queries for _ in range(lax.axis_size("tp"))])
+    piece_now = lax.all_to_all(tile_out, "tp", 0, 0)
+    every_query = jnp.concatenate(piece_now, axis=1)
     seq_count = tokens.shape[0]
     pos_count = cache_keys.shape[2]
     group_size = HEADS // KV_HEADS

time: 128 us -> 127 us (level)
  blocking collectives: 119 us -> 114 us
  starting transfers between devices: 0 us -> 3.38 us
    all_gather x1 -> x0, blocking collectives: 5.19 us -> none  [body(): every_query = lax.all_gather(queries, 'tp', axis=1, tiled=True)]
    all_to_all x0 -> x1, starting transfers between devices: none -> 3.38 us  [body(): piece_now = lax.all_to_all(tile_out, 'tp', 0, 0)]
    unnamed x26 -> x28, local copies, waits for them, and re-layouts: 2.37 us -> 2.86 us
  transfers between devices with their start and end apart: 0 -> 1, of which waited for: 0 -> 1; matrix products, arithmetic and copies ran while one was open for 0% -> 1% of each run, Pallas kernels for 0% -> 0%
where the time goes in v1:
time: 127 us
  blocking collectives  114 us (90%)
  local copies, waits for them, and re-layouts  3.74 us (3%)
  starting transfers between devices  3.38 us (3%)
  other arithmetic  2.19 us (2%)
  matrix products  1.86 us (1%)
  between operations  1.47 us (1%)
    pmax x1, blocking collectives, body(): peak_used = lax.pmax(local_peak, ('kv', 'tp'))  36.9 us
    psum x1, blocking collectives, body(): totals, summed = lax.psum((totals, summed), 'kv')  35.6 us
    psum x1, blocking collectives, body(): lax.psum((jnp.sum(floats * floats, axis=1), query_part, key_part, value_p...  23.6 us
    unnamed x1, blocking collectives  11.7 us
    psum x1, blocking collectives, body(): attended = lax.psum(partial_out.astype(jnp.bfloat16), 'tp')  6.24 us
    all_to_all x1, starting transfers between devices, body(): piece_now = lax.all_to_all(tile_out, 'tp', 0, 0)  3.38 us
    unnamed x28, local copies, waits for them, and re-layouts  2.86 us
  transfers between devices with their start and end apart: 1, of which 1 were waited for; matrix products, arithmetic and copies ran while one was open for 1% of the time, Pallas kernels for 0%

profile of v1, /device:TPU:0, one launch (start us, length us, event | category | flops | bytes accessed | tf_op | source)
XLA Modules:
  0.0 126.9 jit_solution(10512281158984263683)
XLA Ops:
  0.7 0.9 fusion.11
  1.5 0.2 copy-done
  1.7 0.9 fusion.24
  2.6 23.6 %all-reduce.3 = (f32[4,512]{1,0:T(4,128)S(1)}, f32[4]{0:T(128)S(1)}) all-reduce(f32[4,512]{1,0:T(4,128)S(1)} %fusion.24, f32[4]{0:T(128)S(1)} %fusion.11), channel_id=1, replica_groups=mesh['kv'=8,'tp'=4] {'kv'}, use_global_device_ids=true, to_apply=%region_0.0 | all-reduce | flops 2052 | bytes 16416 | tf_op jit(solution)/shard_map/psum | solution.py:32
  26.3 0.6 stack.2
  26.9 3.4 %all-to-all-start = ((bf16[4,4,512]{2,1,0:T(4,128)(2,1)}), bf16[4,4,512]{2,1,0:T(4,128)(2,1)S(1)}, u32[]{:S(2)}, u32[]{:S(2)}) async-start(bf16[4,4,512]{2,1,0:T(4,128)(2,1)} %stack.2), calls=%async_computation | async-start | bytes 32768 | tf_op jit(solution)/shard_map/all_to_all | solution.py:40
  30.4 0.1 fusion.20
  30.5 0.1 fusion.22
  30.6 0.5 copy-done.7
  31.3 0.6 copy-done.9
  31.9 0.2 copy.22
  32.1 0.6 copy-done.11
  32.8 0.6 dynamic-slice
  34.0 0.1 all-to-all-done
  34.3 0.3 fusion.27
  34.5 36.9 %pmax.7 = f32[4,2,8,2]{2,3,1,0:T(2,128)S(1)} all-reduce(f32[4,2,8,2]{2,3,1,0:T(2,128)S(1)} %get-tuple-element.15), channel_id=1, replica_groups=mesh['kv'=8,'tp'=4] {'kv','tp'}, use_global_device_ids=true, to_apply=%region_4.0 | all-reduce | flops 128 | bytes 1024 | tf_op jit(solution)/shard_map/pmax | solution.py:56
  71.4 0.2 fusion.3
  71.8 0.3 convolution_convert_fusion
  72.0 11.7 %all-reduce.4 = (bf16[4,16,2,128]{3,1,2,0:T(8,128)(2,1)S(1)}, bf16[4,16,2]{1,2,0:T(2,128)(2,1)S(1)}) all-reduce(bf16[4,16,2,128]{3,1,2,0:T(8,128)(2,1)S(1)} %bitcast.70, bf16[4,16,2]{1,2,0:T(2,128)(2,1)S(1)} %convert_element_type.51), channel_id=2, replica_groups=mesh['kv'=8,'tp'=4] {'tp'}, use_global_device_ids=true, to_apply=%region_5.6.clone | all-reduce | flops 16512 | bytes 66048
  83.9 35.6 %all-reduce.2 = (f32[4,4,2,128]{3,1,2,0:T(4,128)S(1)}, f32[4,4,2]{1,2,0:T(2,128)S(1)}, f32[4,64]{1,0:T(4,128)S(1)}, f32[4,64]{1,0:T(4,128)S(1)}) all-reduce(f32[4,4,2,128]{3,1,2,0:T(4,128)S(1)} %dynamic-slice_convert_fusion, f32[4,4,2]{1,2,0:T(2,128)S(1)} %dynamic-slice_convert_fusion.1, ...), channel_id=1, replica_groups=mesh['kv'=8,'tp'=4] {'kv'}, use_global_device_ids=true, to_apply=%region_6.7 | all-reduce | flops 4640 | bytes 37120 | tf_op jit(solution)/shard_map/psum | solution.py:73
  119.6 0.2 fusion.16
  119.9 0.2 convolution_convert_fusion.1
  120.0 6.2 %psum.53 = bf16[4,512]{1,0:T(4,128)(2,1)} all-reduce(bf16[4,512]{1,0:T(4,128)(2,1)S(1)} %convolution_convert_fusion.1), channel_id=1, replica_groups=mesh['kv'=8,'tp'=4] {'tp'}, use_global_device_ids=true, to_apply=%region_11.12 | all-reduce | flops 2048 | bytes 8192 | tf_op jit(solution)/shard_map/psum | solution.py:79
  126.3 0.6 multiply_convert_fusion.1
  (36 shorter events, 0.8 us)
Async XLA Ops:
  0.6 1.1 copy-start
  0.6 1.1 copy-start.3
  1.7 30.2 %copy-start.2 = (bf16[4,2,192,128]{3,2,1,0:T(8,128)(2,1)S(1)}, bf16[4,2,192,128]{3,2,1,0:T(8,128)(2,1)}, u32[]{:S(2)}) copy-start(bf16[4,2,192,128]{3,2,1,0:T(8,128)(2,1)} %param.16) | copy-start | bytes 1179652
  2.6 27.8 %copy-start.4 = (bf16[512,64]{0,1:T(8,128)(2,1)S(1)}, bf16[512,64]{0,1:T(8,128)(2,1)}, u32[]{:S(2)}) copy-start(bf16[512,64]{0,1:T(8,128)(2,1)} %param.15) | copy-start | bytes 196612
  26.3 4.0 %copy-start.6 = (f32[512]{0:T(512)S(1)}, f32[512]{0:T(512)}, u32[]{:S(2)}) copy-start(f32[512]{0:T(512)} %param.12) | copy-start | bytes 6148
  26.9 3.6 %copy-start.5 = (bf16[512,64]{0,1:T(8,128)(2,1)S(1)}, bf16[512,64]{0,1:T(8,128)(2,1)}, u32[]{:S(2)}) copy-start(bf16[512,64]{0,1:T(8,128)(2,1)} %param.14) | copy-start | bytes 196612
  26.9 7.2 %all-to-all-start = ((bf16[4,4,512]{2,1,0:T(4,128)(2,1)}), bf16[4,4,512]{2,1,0:T(4,128)(2,1)S(1)}, u32[]{:S(2)}, u32[]{:S(2)}) async-start(bf16[4,4,512]{2,1,0:T(4,128)(2,1)} %stack.2), calls=%async_computation | async-start | bytes 32768 | tf_op jit(solution)/shard_map/all_to_all | solution.py:40
  30.5 0.7 copy-start.7
  30.5 0.7 copy-start.8
  31.2 0.7 copy-start.9
  32.1 0.7 copy-start.11
  34.3 37.5 %copy-start.10 = (bf16[4,2,192,128]{3,2,1,0:T(8,128)(2,1)S(1)}, bf16[4,2,192,128]{3,2,1,0:T(8,128)(2,1)}, u32[]{:S(2)}) copy-start(bf16[4,2,192,128]{3,2,1,0:T(8,128)(2,1)} %param.17) | copy-start | bytes 1179652
  71.6 48.2 %copy-start.1 = (bf16[512,512]{1,0:T(8,128)(2,1)S(1)}, bf16[512,512]{1,0:T(8,128)(2,1)}, u32[]{:S(2)}) copy-start(bf16[512,512]{1,0:T(8,128)(2,1)} %param.21) | copy-start | bytes 1572868
